TPU v7x, 32 devices: a whole 2x2x4 slice. The times are simulated.
32 devices in a mesh: sp: 8 (over z, y), tp: 4 (over x, core).
Axes of the slice: x: 2, y: 2, z: 4, core: 2. Of those that a mesh axis runs over, the one named last changes fastest.
Arguments:
- tokens: bfloat16 [1536, 2048], P('sp', 'tp'), may hold values from -6 to 6
- norm_gain: float32 [2048], replicated, may hold values from 0.1 to 1.9
- query_weight: bfloat16 [2048, 512], P('sp', 'tp'), may hold values from -0.125 to 0.125
- key_weight: bfloat16 [2048, 512], P('sp', 'tp'), may hold values from -0.125 to 0.125
- value_weight: bfloat16 [2048, 512], P('sp', 'tp'), may hold values from -0.125 to 0.125
- decay_weight: bfloat16 [2048, 512], P('sp', 'tp'), may hold values from -0.09375 to 0.09375
- removal_weight: bfloat16 [2048, 512], P('sp', 'tp'), may hold values from -0.125 to 0.125
- gate_weight: bfloat16 [2048, 512], P('sp', 'tp'), may hold values from -0.125 to 0.125
- key_gain: float32 [512], P('tp'), may hold values from 0.1 to 1.9
- removal_gain: float32 [512], P('tp'), may hold values from 0.1 to 1.9
- removal_bias: float32 [512], P('tp'), may hold values from -9 to 1
- decay_bias: float32 [512], P('tp'), may hold values from -12.7 to -1.8
- decay_extra: float32 [1536, 512], P('sp', 'tp'), may hold values from 0 to 0.7
- scan_norm_gain: float32 [512], P('tp'), may hold values from 0.1 to 1.9
- conv_value_weight: bfloat16 [2048, 512], P('sp', 'tp'), may hold values from -0.125 to 0.125
- conv_gate_weight: bfloat16 [2048, 512], P('sp', 'tp'), may hold values from -0.125 to 0.125
- conv_kernel: float32 [31, 512], P(None, 'tp'), may hold values from -2 to 2
- conv_bias: float32 [512], P('tp'), may hold values from -2 to 3
- conv_norm_gain: float32 [512], P('tp'), may hold values from 0.1 to 1.9
- out_scan_weight: bfloat16 [512, 2048], P('tp', 'sp'), may hold values from -0.1875 to 0.1875
- out_conv_weight: bfloat16 [512, 2048], P('tp', 'sp'), may hold values from -0.1875 to 0.1875
Outputs:
- mixed: bfloat16 [1536, 2048], P('sp', 'tp')
All inputs are finite; a program needn't handle non-finite values.
Results may differ from a plain program's by a relative error of at most 0.0073.
Values may be sent and summed in bfloat16 or wider, within the bound.
A program may use at most 64 MiB of HBM per device.

v0:
```python
import jax
import jax.numpy as jnp
from jax import lax
from jax.sharding import PartitionSpec as P

HEAD_SIZE = 64
CONV_K = 31
BLOCK = 32


exact_setting = lax.Precision.HIGHEST


def carried_in(part, axis, combine, identity):
    place = lax.axis_index(axis)
    gathered = jax.tree.map(lambda a: lax.all_gather(a, axis), part)
    state = jax.tree.map(lambda a, e: jnp.zeros_like(a) + jnp.asarray(e, a.dtype), part, identity)

    def one(step, state):
        return combine(
            state, jax.tree.map(lambda a: lax.dynamic_index_in_dim(a, step, 0, False), gathered)
        )

    return lax.fori_loop(0, place, one, state)


def shifted(value, axis, steps):
    count = lax.axis_size(axis)
    leading, last = (max(0, -steps), min(count, count - steps))
    return lax.ppermute(value, axis, [(source, source + steps) for source in range(leading, last)])


def fold_rows(normed, pieces):
    return tuple((jnp.dot(normed, piece, preferred_element_type=jnp.float32) for piece in pieces))


def stored_floats(sums):
    rounded = lax.optimization_barrier(tuple((item.astype(jnp.bfloat16) for item in sums)))
    return tuple((item.astype(jnp.float32) for item in rounded))


def combine_states(earlier, later):
    first = jnp.einsum("hij,hjk->hik", later[0], earlier[0], precision=exact_setting)
    second = jnp.einsum("hij,hjk->hik", later[0], earlier[1], precision=exact_setting) + later[1]
    return (first, second)


def block_product(left, right):
    return jnp.einsum("nhij,nhjk->nhik", left, right, precision=exact_setting)


def pairwise(left, right):
    return jnp.einsum("nhtk,nhik->nhti", left, right, precision=exact_setting)


def scan_mixer(sums, key_gain, removal_gain, removal_bias, decay_bias, decay_extra, scan_norm_gain):
    recept, key_rows, value_rows, decay_pre, removal_pre, gate_pre = stored_floats(sums)
    length = recept.shape[0]
    head_count = recept.shape[1] // HEAD_SIZE
    block_count = length // BLOCK
    decay_rate = jnp.exp(-jax.nn.softplus(-(decay_bias + decay_pre)) - 0.5) + decay_extra
    removal = jax.nn.sigmoid(removal_bias + removal_pre)
    scaled = (key_rows * key_gain).reshape(length, head_count, HEAD_SIZE)
    unit_keys = (
        scaled * lax.rsqrt(jnp.sum(scaled * scaled, axis=-1, keepdims=True) + 1e-06)
    ).reshape(length, -1)
    written = key_rows * (1.0 + (removal - 1.0) * removal_gain)

    def blocked(table):
        return table.reshape(block_count, BLOCK, head_count, HEAD_SIZE).transpose(0, 2, 1, 3)

    recept_b = blocked(recept)
    written_b = blocked(written)
    values_b = blocked(value_rows)
    rate_b = blocked(decay_rate)
    unit_b = blocked(unit_keys)
    removal_b = blocked(removal)
    falling = -jnp.cumsum(rate_b, axis=2)
    before = falling + rate_b
    middle = falling[:, :, BLOCK // 2 : BLOCK // 2 + 1]
    ending = falling[:, :, BLOCK - 1 :]
    alpha = -unit_b
    beta = unit_b * removal_b
    position = jnp.arange(BLOCK)
    strict = (position[:, None] > position[None, :]).astype(jnp.float32)
    inclusive = (position[:, None] >= position[None, :]).astype(jnp.float32)
    alpha_mid = alpha * jnp.exp(before - middle)
    recept_mid = recept_b * jnp.exp(falling - middle)
    beta_mid = beta * jnp.exp(middle - falling)
    keys_mid = written_b * jnp.exp(middle - falling)
    alpha_beta = pairwise(alpha_mid, beta_mid) * strict
    alpha_keys = pairwise(alpha_mid, keys_mid) * strict
    recept_beta = pairwise(recept_mid, beta_mid) * inclusive
    recept_keys = pairwise(recept_mid, keys_mid) * inclusive
    inverse = jnp.eye(BLOCK, dtype=jnp.float32) + alpha_beta
    power = alpha_beta
    for index in range(BLOCK.bit_length() - 2):
        power = block_product(power, power)
        inverse = inverse + block_product(inverse, power)
    widened = jnp.concatenate([values_b, jnp.zeros_like(values_b)], axis=-1)
    rhs_local = block_product(alpha_keys, widened)
    read_local = block_product(recept_keys, widened)
    start_alpha = alpha * jnp.exp(before)
    start_recept = recept_b * jnp.exp(falling)
    end_beta = beta * jnp.exp(ending - falling)
    end_keys = written_b * jnp.exp(ending - falling)
    end_decay = jnp.exp(ending)[:, :, 0, :]

    def advance(carried_state, inputs):
        (
            starting_alpha,
            starting_receptance,
            solver,
            r_beta,
            r_local,
            right_operand,
            ending_beta,
            ending_key_rows,
            e_decay,
            widen_width,
        ) = inputs
        gathered_rows = (
            jnp.einsum("qfl,qlz->qfz", starting_alpha, carried_state, precision=exact_setting)
            + right_operand
        )
        removed_value = jnp.einsum("hti,hiv->htv", solver, gathered_rows, precision=exact_setting)
        readout = (
            jnp.einsum("qfl,qlz->qfz", starting_receptance, carried_state, precision=exact_setting)
            + jnp.einsum("hti,hiv->htv", r_beta, removed_value, precision=exact_setting)
            + r_local
        )
        carried_state = (
            e_decay[:, :, None] * carried_state
            + jnp.einsum("pzw,pzb->pwb", ending_beta, removed_value, precision=exact_setting)
            + jnp.einsum("pzw,pzb->pwb", ending_key_rows, widen_width, precision=exact_setting)
        )
        return (carried_state, readout)

    identity = jnp.broadcast_to(
        jnp.eye(HEAD_SIZE, dtype=jnp.float32), (head_count, HEAD_SIZE, HEAD_SIZE)
    )
    initial = jnp.concatenate([jnp.zeros_like(identity), identity], axis=-1)
    final, readout_rows = lax.scan(
        advance,
        initial,
        (
            start_alpha,
            start_recept,
            inverse,
            recept_beta,
            read_local,
            rhs_local,
            end_beta,
            end_keys,
            end_decay,
            widened,
        ),
    )
    incoming_state = carried_in(
        (final[:, :, HEAD_SIZE:], final[:, :, :HEAD_SIZE]),
        "sp",
        combine_states,
        (identity, jnp.zeros_like(identity)),
    )
    reads = readout_rows[..., :HEAD_SIZE] + jnp.einsum(
        "yqem,qmb->yqeb", readout_rows[..., HEAD_SIZE:], incoming_state[1], precision=exact_setting
    )
    reads = reads.transpose(0, 2, 1, 3).reshape(length, head_count, HEAD_SIZE)
    center = jnp.mean(reads, axis=-1, keepdims=True)
    spread = jnp.mean((reads - center) ** 2, axis=-1, keepdims=True)
    normalized = ((reads - center) * lax.rsqrt(spread + 0.00064)).reshape(length, -1)
    return (normalized * scan_norm_gain * jax.nn.sigmoid(gate_pre)).astype(jnp.bfloat16)


def conv_mixer(sums, conv_kernel, conv_bias, conv_norm_gain):
    value_part, gate_part = stored_floats(sums)
    conv_input = (value_part * jax.nn.sigmoid(gate_part)).astype(jnp.bfloat16)
    length = conv_input.shape[0]
    rim = shifted(conv_input[length - (CONV_K - 1) :], "sp", 1)
    padded = jnp.concatenate([rim, conv_input], axis=0).astype(jnp.float32)
    filtered = conv_bias + conv_kernel[0] * padded[0:length]
    for index in range(1, CONV_K):
        filtered = filtered + conv_kernel[index] * padded[index : index + length]
    totals = lax.psum((jnp.sum(filtered, axis=-1), jnp.sum(filtered * filtered, axis=-1)), "tp")
    channels = filtered.shape[1] * lax.axis_size("tp")
    center = totals[0] / channels
    spread = totals[1] / channels - center * center
    scaled = (filtered - center[:, None]) * lax.rsqrt(spread[:, None] + 1e-05) * conv_norm_gain
    return jax.nn.silu(scaled).astype(jnp.bfloat16)


def shards(
    tokens,
    norm_gain,
    query_weight,
    key_weight,
    value_weight,
    decay_weight,
    removal_weight,
    gate_weight,
    key_gain,
    removal_gain,
    removal_bias,
    decay_bias,
    decay_extra,
    scan_norm_gain,
    conv_value_weight,
    conv_gate_weight,
    conv_kernel,
    conv_bias,
    conv_norm_gain,
    out_scan_weight,
    out_conv_weight,
):
    stacked = jnp.concatenate([out_scan_weight, out_conv_weight], axis=0)
    all_columns = lax.all_gather(stacked, "sp", axis=1, tiled=True)
    regrouped = lax.all_to_all(all_columns, "tp", split_axis=1, concat_axis=0, tiled=True)
    whole = lax.all_gather(tokens, "tp", axis=1, tiled=True)
    floats = whole.astype(jnp.float32)
    normed = (
        floats * lax.rsqrt(jnp.mean(floats * floats, axis=-1, keepdims=True) + 1e-06) * norm_gain
    ).astype(jnp.bfloat16)
    projected = fold_rows(
        normed,
        (
            lax.all_gather(query_weight, "sp", axis=0, tiled=True),
            lax.all_gather(key_weight, "sp", axis=0, tiled=True),
            lax.all_gather(value_weight, "sp", axis=0, tiled=True),
            lax.all_gather(decay_weight, "sp", axis=0, tiled=True),
            lax.all_gather(removal_weight, "sp", axis=0, tiled=True),
            lax.all_gather(gate_weight, "sp", axis=0, tiled=True),
            lax.all_gather(conv_value_weight, "sp", axis=0, tiled=True),
            lax.all_gather(conv_gate_weight, "sp", axis=0, tiled=True),
        ),
    )
    scan_sums = projected[:6]
    conv_sums = projected[6:]
    scan_out = scan_mixer(
        scan_sums, key_gain, removal_gain, removal_bias, decay_bias, decay_extra, scan_norm_gain
    )
    conv_out = conv_mixer(conv_sums, conv_kernel, conv_bias, conv_norm_gain)
    features = jnp.concatenate([scan_out, conv_out], axis=1)
    mixer_all = lax.all_gather(features, "tp", axis=1, tiled=True)
    summed = jnp.dot(mixer_all, regrouped, preferred_element_type=jnp.float32)
    return summed.astype(jnp.bfloat16)


def solution(mesh):
    placed = (
        P("sp", "tp"),
        P(),
        P("sp", "tp"),
        P("sp", "tp"),
        P("sp", "tp"),
        P("sp", "tp"),
        P("sp", "tp"),
        P("sp", "tp"),
        P("tp"),
        P("tp"),
        P("tp"),
        P("tp"),
        P("sp", "tp"),
        P("tp"),
        P("sp", "tp"),
        P("sp", "tp"),
        P(None, "tp"),
        P("tp"),
        P("tp"),
        P("tp", "sp"),
        P("tp", "sp"),
    )
    return jax.shard_map(
        shards, mesh=mesh, in_specs=placed, out_specs=P("sp", "tp"), check_vma=False
    )
```

profile of v0, /device:TPU:0, one launch (start us, length us, event | category | flops | bytes accessed | tf_op | source)
XLA Modules:
  0.0 395.4 jit_solution(8425970206136668507)
XLA Ops:
  6.5 33.4 %all_gather.56 = bf16[2048,128]{1,0:T(8,128)(2,1)S(1)} all-gather(bf16[256,128]{1,0:T(8,128)(2,1)} %param.39), channel_id=1, replica_groups=mesh['sp'=8,'tp'=4] {'sp'}, dimensions={0}, use_global_device_ids=true | all-gather | bytes 589824 | tf_op jit(solution)/shard_map/all_gather | solution.py:232
  39.9 8.9 %all_gather.45 = bf16[192,2048]{1,0:T(8,128)(2,1)S(1)} all-gather(bf16[192,512]{1,0:T(8,128)(2,1)} %param.25), channel_id=1, replica_groups=mesh['sp'=8,'tp'=4] {'tp'}, dimensions={1}, use_global_device_ids=true | all-gather | bytes 983040 | tf_op jit(solution)/shard_map/all_gather | solution.py:218
  48.8 0.2 fusion.29
  49.1 31.2 %all_gather.57 = bf16[2048,128]{1,0:T(8,128)(2,1)S(1)} all-gather(bf16[256,128]{1,0:T(8,128)(2,1)S(1)} %copy-done.1), channel_id=1, replica_groups=mesh['sp'=8,'tp'=4] {'sp'}, dimensions={0}, use_global_device_ids=true | all-gather | bytes 589824 | tf_op jit(solution)/shard_map/all_gather | solution.py:233
  80.3 0.4 convolution_convert_fusion.2
  80.8 0.4 convolution_convert_fusion.1
  81.3 3.6 collective-permute-start
  85.2 0.7 pad_maximum_fusion
  86.0 32.5 %all_gather.46 = bf16[2048,128]{1,0:T(8,128)(2,1)S(1)} all-gather(bf16[256,128]{1,0:T(8,128)(2,1)S(1)} %copy-done.2), channel_id=1, replica_groups=mesh['sp'=8,'tp'=4] {'sp'}, dimensions={0}, use_global_device_ids=true | all-gather | bytes 589824 | tf_op jit(solution)/shard_map/all_gather | solution.py:226
  118.4 0.4 convolution_convert_fusion.8
  118.9 0.4 copy-done.3
  119.3 31.8 %all_gather.47 = bf16[2048,128]{1,0:T(8,128)(2,1)S(1)} all-gather(bf16[256,128]{1,0:T(8,128)(2,1)S(1)} %copy-done.3), channel_id=1, replica_groups=mesh['sp'=8,'tp'=4] {'sp'}, dimensions={0}, use_global_device_ids=true | all-gather | bytes 589824 | tf_op jit(solution)/shard_map/all_gather | solution.py:227
  151.0 0.4 convolution_convert_fusion.7
  151.5 0.4 copy-done.4
  151.9 31.6 %all_gather.48 = bf16[2048,128]{1,0:T(8,128)(2,1)S(1)} all-gather(bf16[256,128]{1,0:T(8,128)(2,1)S(1)} %copy-done.4), channel_id=1, replica_groups=mesh['sp'=8,'tp'=4] {'sp'}, dimensions={0}, use_global_device_ids=true | all-gather | bytes 589824 | tf_op jit(solution)/shard_map/all_gather | solution.py:228
  183.4 0.4 convolution_convert_fusion.6
  183.9 0.4 copy-done.5
  184.3 31.3 %all_gather.49 = bf16[2048,128]{1,0:T(8,128)(2,1)S(1)} all-gather(bf16[256,128]{1,0:T(8,128)(2,1)S(1)} %copy-done.5), channel_id=1, replica_groups=mesh['sp'=8,'tp'=4] {'sp'}, dimensions={0}, use_global_device_ids=true | all-gather | bytes 589824 | tf_op jit(solution)/shard_map/all_gather | solution.py:229
  215.6 0.4 convolution_convert_fusion.5
  216.0 0.4 copy-done.6
  216.4 31.5 %all_gather.50 = bf16[2048,128]{1,0:T(8,128)(2,1)S(1)} all-gather(bf16[256,128]{1,0:T(8,128)(2,1)S(1)} %copy-done.6), channel_id=1, replica_groups=mesh['sp'=8,'tp'=4] {'sp'}, dimensions={0}, use_global_device_ids=true | all-gather | bytes 589824 | tf_op jit(solution)/shard_map/all_gather | solution.py:230
  247.9 0.4 convolution_convert_fusion.4
  248.3 0.4 copy-done.7
  248.7 31.6 %all_gather.51 = bf16[2048,128]{1,0:T(8,128)(2,1)S(1)} all-gather(bf16[256,128]{1,0:T(8,128)(2,1)S(1)} %copy-done.7), channel_id=1, replica_groups=mesh['sp'=8,'tp'=4] {'sp'}, dimensions={0}, use_global_device_ids=true | all-gather | bytes 589824 | tf_op jit(solution)/shard_map/all_gather | solution.py:231
  280.3 0.4 convolution_convert_fusion.3
  280.8 0.4 copy-done
  281.6 0.2 reduce_window_sum.11
  282.7 0.5 convolution_multiply_fusion.2
  283.4 0.5 convolution_multiply_fusion.3
  283.9 0.5 convolution_multiply_fusion.1
  284.4 0.5 convolution_multiply_fusion
  285.0 0.3 fusion.101
  285.3 0.3 fusion.102
  285.7 0.3 convolution_add_fusion.8
  286.0 0.3 fusion.103
  286.3 0.3 convolution_add_fusion.7
  286.6 0.3 fusion.104
  287.0 0.3 convolution_add_fusion.6
  287.4 0.2 fusion.74
  287.7 0.2 fusion.72
  287.9 0.3 convolution_add_fusion.5
  288.2 8.3 %while.24 = (s32[]{:T(128)}, f32[2,64,128]{2,1,0:T(8,128)S(1)}, f32[6,2,32,128]{3,2,0,1:T(8,128)S(1)}, f32[6,2,64]{2,1,0:T(2,128)S(1)}, f32[6,2,32,64]{3,2,1,0:T...) while((s32[]{:T(128)}, f32[2,64,128]{2,1,0:T(8,128)S(1)}, ...), condition=%wide.region_4.5_spmd, body=%wide.region_3.4_spmd.sunk | while | flops 31531008 | bytes 955549 | solution.py:143
  288.8 0.3 convolution_add_fusion.14
  289.1 0.3 convolution_add_fusion.15
  290.2 0.3 convolution_add_fusion.14
  290.5 0.3 convolution_add_fusion.15
  291.5 0.3 convolution_add_fusion.14
  291.8 0.3 convolution_add_fusion.15
  292.9 0.3 convolution_add_fusion.14
  293.2 0.3 convolution_add_fusion.15
  294.3 0.3 convolution_add_fusion.14
  294.6 0.3 convolution_add_fusion.15
  295.7 0.3 convolution_add_fusion.14
  296.0 0.3 convolution_add_fusion.15
  296.6 31.2 %all-gather = f32[16,64,64]{2,1,0:T(8,128)S(1)} all-gather(f32[2,64,64]{2,1,0:T(8,128)S(1)} %get-tuple-element.186), channel_id=2, replica_groups=mesh['sp'=8,'tp'=4] {'sp'}, dimensions={0}, use_global_device_ids=true | all-gather | bytes 294912 | tf_op jit(solution)/shard_map/all_gather | solution.py:16
  327.7 31.2 %all-gather.1 = f32[16,64,64]{2,1,0:T(8,128)S(1)} all-gather(f32[2,64,64]{2,1,0:T(8,128)S(1)} %get-tuple-element.185), channel_id=3, replica_groups=mesh['sp'=8,'tp'=4] {'sp'}, dimensions={0}, use_global_device_ids=true | all-gather | bytes 294912 | tf_op jit(solution)/shard_map/all_gather | solution.py:16
  359.1 0.5 fusion.100
  359.8 0.2 multiply_reduce_fusion
  360.7 3.5 all-to-all-start
  364.3 0.5 fusion.96
  364.8 15.4 %all-reduce.2 = (f32[192]{0:T(256)S(1)}, f32[192]{0:T(256)S(1)}) all-reduce(f32[192]{0:T(256)S(1)} %get-tuple-element.137, f32[192]{0:T(256)S(1)} %get-tuple-element.136), channel_id=1, replica_groups=mesh['sp'=8,'tp'=4] {'tp'}, use_global_device_ids=true, to_apply=%region_12.13 | all-reduce | flops 384 | bytes 3072 | tf_op jit(solution)/shard_map/psum | solution.py:184
  380.3 6.6 %all_gather.58 = bf16[192,1024]{1,0:T(8,128)(2,1)S(1)} all-gather(bf16[192,256]{1,0:T(8,128)(2,1)S(1)} %pad_maximum_fusion.1), channel_id=1, replica_groups=mesh['sp'=8,'tp'=4] {'tp'}, dimensions={1}, use_global_device_ids=true | all-gather | bytes 491520 | tf_op jit(solution)/shard_map/all_gather | solution.py:243
  386.9 0.5 copy.77
  387.5 1.1 convolution_convert_fusion
  (117 shorter events, 7.4 us)
Async XLA Ops:
  6.5 42.5 %copy-start.1 = (bf16[256,128]{1,0:T(8,128)(2,1)S(1)}, bf16[256,128]{1,0:T(8,128)(2,1)}, u32[]{:S(2)}) copy-start(bf16[256,128]{1,0:T(8,128)(2,1)} %param.40) | copy-start | bytes 196612
  6.5 354.2 %all-gather.4.cloned.1.call-start = ((), (), s32[]{:S(2)}) async-start(), calls=%async_computation.1 | async-start | bytes 1179648 | tf_op jit(solution)/shard_map/all_gather | solution.py:216
  39.9 40.4 %copy-start.18 = (f32[2048]{0:T(1024)S(1)}, f32[2048]{0:T(1024)}, u32[]{:S(2)}) copy-start(f32[2048]{0:T(1024)} %param.26) | copy-start | bytes 24580
  80.8 4.2 %copy-start.8 = (bf16[128,256]{1,0:T(8,128)(2,1)S(1)}, bf16[128,256]{1,0:T(8,128)(2,1)}, u32[]{:S(2)}) copy-start(bf16[128,256]{1,0:T(8,128)(2,1)} %param.45) | copy-start | bytes 196612
  80.8 4.3 %copy-start.9 = (bf16[128,256]{1,0:T(8,128)(2,1)S(1)}, bf16[128,256]{1,0:T(8,128)(2,1)}, u32[]{:S(2)}) copy-start(bf16[128,256]{1,0:T(8,128)(2,1)} %param.44) | copy-start | bytes 196612
  80.8 5.2 %copy-start.2 = (bf16[256,128]{1,0:T(8,128)(2,1)S(1)}, bf16[256,128]{1,0:T(8,128)(2,1)}, u32[]{:S(2)}) copy-start(bf16[256,128]{1,0:T(8,128)(2,1)} %param.27) | copy-start | bytes 196612
  81.3 279.4 %collective-permute-start = (bf16[30,128]{1,0:T(8,128)(2,1)S(1)}, bf16[30,128]{1,0:T(8,128)(2,1)S(1)}, u32[]{:S(2)}, u32[]{:S(2)}) collective-permute-start(bf16[30,128]{1,0:T(8,128)(2,1)S(1)} %slice.278), channel_id=1, source_target_pairs={{0,4},{4,8},{8,12},{12,16},{16,20},{20,24},{24,28},{1,5},{5,9},{9,... | collective-permute-start | bytes 23048 | tf_op jit(solution)/shard_map/ppermute | solution.py:30
  118.4 0.8 copy-start.3
  151.0 0.8 copy-start.4
  183.4 0.8 copy-start.5
  215.6 0.8 copy-start.6
  247.9 0.8 copy-start.7
  280.3 0.9 copy-start
  280.3 0.9 copy-start.13
  280.3 0.9 copy-start.14
  280.3 0.9 copy-start.15
  280.3 0.9 copy-start.16
  359.1 1.5 copy-start.10
  359.1 1.5 copy-start.11
  360.7 3.5 copy-start.17
  360.7 26.2 %all-to-all-start = ((bf16[256,4,512]{0,2,1:T(8,128)(2,1)}), bf16[256,4,512]{0,2,1:T(8,128)(2,1)S(1)}, u32[]{:S(2)}, u32[]{:S(2)}) async-start(bf16[256,4,512]{0,2,1:T(8,128)(2,1)} %bitcast.243), calls=%async_computation | async-start | bytes 2097152 | tf_op jit(solution)/shard_map/all_to_all | solution.py:217
  364.3 15.9 %copy-start.12 = (f32[128]{0:T(128)S(1)}, f32[128]{0:T(128)}, u32[]{:S(2)}) copy-start(f32[128]{0:T(128)} %param.43) | copy-start | bytes 1540
Sparse Core Ops, SparseCore 0:
  86.0 41.8 all-gather.3
where the time goes:
time: 396 us; the launch traced here: 395 us
  blocking collectives  348 us (88%)
  matrix products  17.8 us (4%)
  between operations  14 us (4%)
  starting transfers between devices  7.14 us (2%)
  local copies, waits for them, and re-layouts  5.31 us (1%)
    all_gather x2, blocking collectives, carried_in(): gathered = jax.tree.map(lambda a: lax.all_gather(a, axis), part)  62.3 us
    all_gather x1, blocking collectives, shards(): lax.all_gather(conv_value_weight, 'sp', axis=0, tiled=True)  33.4 us
    all_gather x1, blocking collectives, shards(): lax.all_gather(query_weight, 'sp', axis=0, tiled=True)  32.5 us
    all_gather x1, blocking collectives, shards(): lax.all_gather(key_weight, 'sp', axis=0, tiled=True)  31.8 us
    all_gather x1, blocking collectives, shards(): lax.all_gather(gate_weight, 'sp', axis=0, tiled=True)  31.6 us
    all_gather x1, blocking collectives, shards(): lax.all_gather(value_weight, 'sp', axis=0, tiled=True)  31.6 us
    all_gather x1, blocking collectives, shards(): lax.all_gather(removal_weight, 'sp', axis=0, tiled=True)  31.5 us
    all_gather x1, blocking collectives, shards(): lax.all_gather(decay_weight, 'sp', axis=0, tiled=True)  31.3 us
  transfers between devices with their start and end apart: 3, of which 0 were waited for; matrix products, arithmetic and copies ran while one was open for 5% of the time, Pallas kernels for 0%

commit v1 on v0

v1 whole, which is shorter than its diff:
```python
import functools

import jax
import jax.numpy as jnp
from jax import lax
from jax.experimental import pallas as pl
from jax.experimental.pallas import tpu as pltpu
from jax.sharding import PartitionSpec as P

HEAD_SIZE = 64
CONV_K = 31
HALO = 32
BLOCK = 32
SEGMENT = 96
MESH = pl.DeviceIdType.MESH

exact_setting = lax.Precision.HIGHEST


def remote(src, dst, send, recv, sp, tp):
    return pltpu.make_async_remote_copy(
        src_ref=src, dst_ref=dst, send_sem=send, recv_sem=recv,
        device_id={"sp": sp, "tp": tp}, device_id_type=MESH,
    )


def project_kernel(
    nsp, ntp, tokens, gain, weights, extra, outw,
    proj, extra_all, outw_all,
    tok, normed, full,
    send_y, recv_w, send_up, send_dn, send_tok, recv_tok, send_halo, recv_halo,
    send_out, recv_out, send_fwd, send_ex, recv_ex, local,
):
    s, t = lax.axis_index("sp"), lax.axis_index("tp")
    p, y = s // 2, s % 2
    np_ = nsp // 2
    mate = 2 * p + 1 - y
    rows = tokens.shape[0]
    depth = weights.shape[1]
    group = nsp // ntp
    half = group // 2

    def slot(b):
        return full.at[pl.ds(pl.multiple_of(b * depth, depth), depth), :]

    def place(yy, q):
        return tok.at[q, pl.ds(pl.multiple_of(HALO + yy * rows, 16), rows), :]

    def weight_copy(b, yy, sems, to):
        i = 2 * b + yy
        return remote(slot(i), slot(i), sems.at[i], recv_w.at[i], 2 * to + y, t)

    own = pltpu.make_async_copy(weights.at[y], slot(s), local.at[0])
    own.start()
    swap = remote(weights.at[1 - y], slot(s), send_y.at[0], recv_w.at[s], mate, t)
    swap.start()

    def send_own(sems, to):
        return remote(weights.at[y], slot(s), sems.at[s], recv_w.at[s], 2 * to + y, t)

    @pl.when(p + 1 < np_)
    def _():
        send_own(send_up, p + 1).start()

    @pl.when(p > 0)
    def _():
        send_own(send_dn, p - 1).start()

    mine = pltpu.make_async_copy(tokens, place(y, t), local.at[1])
    mine.start()
    group_size = 2 * ntp
    me = y * ntp + t

    def tok_send(d):
        g = lax.rem(me + d, group_size)
        return remote(tokens, place(y, t), send_tok.at[d], recv_tok.at[me], 2 * p + g // ntp, g % ntp)

    def halo_send(g):
        return remote(
            tokens.at[pl.ds(rows - HALO, HALO), :], tok.at[t, pl.ds(0, HALO), :],
            send_halo.at[g], recv_halo.at[t], 2 * (p + 1) + g // ntp, g % ntp,
        )

    for d in range(1, group_size):
        tok_send(d).start()
    sends_halo = jnp.logical_and(y == 1, p + 1 < np_)

    @pl.when(sends_halo)
    def _():
        for g in range(group_size):
            halo_send(g).start()

    ex_own = pltpu.make_async_copy(extra.at[y], extra_all.at[y], local.at[2])
    ex_own.start()
    ex = remote(extra.at[1 - y], extra_all.at[y], send_ex.at[0], recv_ex.at[0], mate, t)
    ex.start()

    j, q_to = s % group, s // group
    y_to = j // half

    def out_send(k):
        return remote(
            outw, outw_all.at[j, t], send_out.at[k], recv_out.at[j * ntp + t], 2 * k + y_to, q_to
        )

    def is_self(k):
        return jnp.logical_and(2 * k + y_to == s, q_to == t)

    def out_local():
        return pltpu.make_async_copy(outw, outw_all.at[j, t], recv_out.at[j * ntp + t])

    def start_out(k, c):
        @pl.when(is_self(k))
        def _():
            out_local().start()

        @pl.when(jnp.logical_not(is_self(k)))
        def _():
            out_send(k).start()

        return c

    own.wait()
    remote(slot(mate), slot(mate), send_y.at[0], recv_w.at[mate], mate, t).wait_recv()

    @pl.when(p + 1 < np_)
    def _():
        weight_copy(p, 1 - y, send_up, p + 1).start()

    @pl.when(p > 0)
    def _():
        weight_copy(p, 1 - y, send_dn, p - 1).start()

    lax.fori_loop(0, np_, start_out, 0)

    def line(k, c):
        for e in range(2):
            yy = lax.rem(y + e, 2)
            low, high = p - k, p + k

            @pl.when(low >= 0)
            def _():
                weight_copy(low, yy, send_up, p).wait_recv()

                @pl.when(p + 1 < np_)
                def _():
                    weight_copy(low, yy, send_up, p + 1).start()

            @pl.when(high < np_)
            def _():
                weight_copy(high, yy, send_dn, p).wait_recv()

                @pl.when(p > 0)
                def _():
                    weight_copy(high, yy, send_dn, p - 1).start()

        return c

    lax.fori_loop(1, 2, line, 0)

    mine.wait()
    for d in range(1, group_size):
        g = lax.rem(me + d, group_size)
        view = place(g // ntp, g % ntp)
        remote(view, view, send_tok.at[0], recv_tok.at[g], mate, t).wait_recv()

    @pl.when(p > 0)
    def _():
        for q in range(ntp):
            view = tok.at[q, pl.ds(0, HALO), :]
            remote(view, view, send_tok.at[0], recv_halo.at[q], mate, t).wait_recv()

    @pl.when(p == 0)
    def _():
        tok[:, 0:HALO, :] = jnp.zeros((ntp, HALO, tok.shape[2]), tok.dtype)

    width = tok.shape[2]
    total_rows = tok.shape[1]
    tile = HALO

    def norm_tile(i, c):
        at = pl.ds(pl.multiple_of(i * tile, tile), tile)
        squares = jnp.zeros((tile, 1), jnp.float32)
        for q in range(ntp):
            x = tok[q, at, :].astype(jnp.float32)
            squares = squares + jnp.sum(x * x, axis=-1, keepdims=True)
        scale = lax.rsqrt(squares / (ntp * width) + 1e-06)
        for q in range(ntp):
            x = tok[q, at, :].astype(jnp.float32)
            g = gain[:, q * width : (q + 1) * width]
            normed[at, q * width : (q + 1) * width] = (x * scale * g).astype(jnp.bfloat16)
        return c

    lax.fori_loop(0, total_rows // tile, norm_tile, 0)
    lax.fori_loop(2, np_, line, 0)

    def out_view(i):
        return outw_all.at[i // ntp, i % ntp]

    def forward(i):
        return remote(out_view(i), out_view(i), send_fwd.at[i], recv_out.at[i], mate, t)

    base = y * half * ntp
    other = (1 - y) * half * ntp

    def start_forward(i, c):
        forward(base + i).wait_recv()
        forward(base + i).start()
        return c

    lax.fori_loop(0, half * ntp, start_forward, 0)

    columns = full.shape[1]
    for n in range(0, columns, 256):
        proj[:, n : n + 256] = jnp.dot(
            normed[...], full[:, n : n + 256], preferred_element_type=jnp.float32
        ).astype(jnp.bfloat16)

    def end_forward(i, c):
        forward(other + i).wait_recv()
        forward(base + i).wait_send()
        return c

    lax.fori_loop(0, half * ntp, end_forward, 0)
    swap.wait_send()
    ex_own.wait()
    ex.wait()
    for d in range(1, group_size):
        tok_send(d).wait_send()

    @pl.when(sends_halo)
    def _():
        for g in range(group_size):
            halo_send(g).wait_send()

    def end_out(k, c):
        @pl.when(jnp.logical_not(is_self(k)))
        def _():
            out_send(k).wait_send()

        for yy in range(2):

            @pl.when(jnp.logical_and(k <= p, p + 1 < np_))
            def _():
                weight_copy(k, yy, send_up, p).wait_send()

            @pl.when(jnp.logical_and(k >= p, p > 0))
            def _():
                weight_copy(k, yy, send_dn, p).wait_send()

        return c

    lax.fori_loop(0, np_, end_out, 0)


def state_kernel(nsp, ntp, state, stats, states, stats_all, send_st, recv_st, send_g, recv_g, local):
    s, t = lax.axis_index("sp"), lax.axis_index("tp")
    p, y = s // 2, s % 2
    np_ = nsp // 2
    group_size = 2 * ntp
    me = y * ntp + t

    def st(k):
        return remote(state, states.at[p], send_st.at[k], recv_st.at[p], 2 * k + y, t)

    def st_in(k):
        return remote(states.at[k], states.at[k], send_st.at[k], recv_st.at[k], 2 * k + y, t)

    def start(k, c):
        st(k).start()
        return c

    lax.fori_loop(p + 1, np_, start, 0)
    copy = pltpu.make_async_copy(stats, stats_all.at[me], local.at[0])
    copy.start()

    def send(d):
        g = lax.rem(me + d, group_size)
        return remote(stats, stats_all.at[me], send_g.at[d], recv_g.at[me], 2 * p + g // ntp, g % ntp)

    for d in range(1, group_size):
        send(d).start()
    for d in range(1, group_size):
        g = lax.rem(me + d, group_size)
        remote(stats_all.at[g], stats_all.at[g], send_g.at[d], recv_g.at[g], s, t).wait_recv()
        send(d).wait_send()
    copy.wait()

    def end_in(k, c):
        st_in(k).wait_recv()
        return c

    lax.fori_loop(0, p, end_in, 0)

    def end_out(k, c):
        st(k).wait_send()
        return c

    lax.fori_loop(p + 1, np_, end_out, 0)


def feature_kernel(ntp, features, gathered, send_g, recv_g, local):
    s, t = lax.axis_index("sp"), lax.axis_index("tp")
    p, y = s // 2, s % 2
    group_size = 2 * ntp
    me = 2 * t + y
    wide = features.shape[2]

    def columns(g):
        return gathered.at[:, pl.ds(pl.multiple_of(g * wide, 128), wide)]

    copy = pltpu.make_async_copy(features.at[y], columns(me), local.at[0])
    copy.start()

    def send(d):
        g = lax.rem(me + d, group_size)
        return remote(features.at[g % 2], columns(me), send_g.at[d], recv_g.at[me], 2 * p + g % 2, g // 2)

    for d in range(1, group_size):
        send(d).start()
    for d in range(1, group_size):
        g = lax.rem(me + d, group_size)
        remote(columns(g), columns(g), send_g.at[d], recv_g.at[g], s, t).wait_recv()
        send(d).wait_send()
    copy.wait()


def call(kernel, outs, scratch, *operands):
    vmem = pl.BlockSpec(memory_space=pltpu.VMEM)
    return pl.pallas_call(
        kernel,
        out_shape=outs,
        in_specs=[vmem] * len(operands),
        out_specs=jax.tree.map(lambda _: vmem, outs),
        scratch_shapes=scratch,
        compiler_params=pltpu.CompilerParams(
            has_side_effects=True, vmem_limit_bytes=40 * 1024 * 1024
        ),
    )(*operands)


def combine_states(earlier, later):
    first = jnp.einsum("hij,hjk->hik", later[0], earlier[0], precision=exact_setting)
    second = jnp.einsum("hij,hjk->hik", later[0], earlier[1], precision=exact_setting) + later[1]
    return (first, second)


def block_product(left, right):
    return jnp.einsum("nhij,nhjk->nhik", left, right, precision=exact_setting)


def pairwise(left, right):
    return jnp.einsum("nhtk,nhik->nhti", left, right, precision=exact_setting)


def local_scan(recept, key_rows, values, decay_pre, removal_pre, key_gain, removal_gain, removal_bias, decay_bias, decay_extra):
    length = recept.shape[0]
    segments = length // SEGMENT
    steps = SEGMENT // BLOCK
    decay_rate = jnp.exp(-jax.nn.softplus(-(decay_bias + decay_pre)) - 0.5) + decay_extra
    removal = jax.nn.sigmoid(removal_bias + removal_pre)
    scaled = key_rows * key_gain
    unit_keys = scaled * lax.rsqrt(jnp.sum(scaled * scaled, axis=-1, keepdims=True) + 1e-06)
    written = key_rows * (1.0 + (removal - 1.0) * removal_gain)

    def blocked(table):
        return table.reshape(segments, steps, BLOCK, HEAD_SIZE).transpose(1, 0, 2, 3)

    recept_b, written_b, values_b = blocked(recept), blocked(written), blocked(values)
    rate_b, unit_b, removal_b = blocked(decay_rate), blocked(unit_keys), blocked(removal)
    position = jnp.arange(BLOCK)
    strict = (position[:, None] > position[None, :]).astype(jnp.float32)
    inclusive = (position[:, None] >= position[None, :]).astype(jnp.float32)
    falling = -jnp.einsum("ti,nhik->nhtk", inclusive, rate_b, precision=exact_setting)
    before = falling + rate_b
    middle = falling[:, :, BLOCK // 2 : BLOCK // 2 + 1]
    ending = falling[:, :, BLOCK - 1 :]
    alpha = -unit_b
    beta = unit_b * removal_b
    alpha_mid = alpha * jnp.exp(before - middle)
    recept_mid = recept_b * jnp.exp(falling - middle)
    lift = jnp.exp(middle - falling)
    beta_mid = beta * lift
    keys_mid = written_b * lift
    alpha_beta = pairwise(alpha_mid, beta_mid) * strict
    alpha_keys = pairwise(alpha_mid, keys_mid) * strict
    recept_beta = pairwise(recept_mid, beta_mid) * inclusive
    recept_keys = pairwise(recept_mid, keys_mid) * inclusive
    inverse = jnp.eye(BLOCK, dtype=jnp.float32) + alpha_beta
    power = alpha_beta
    for index in range(BLOCK.bit_length() - 2):
        power = block_product(power, power)
        inverse = inverse + block_product(inverse, power)
    widened = jnp.concatenate([values_b, jnp.zeros_like(values_b)], axis=-1)
    rhs_local = block_product(alpha_keys, widened)
    read_local = block_product(recept_keys, widened)
    start_alpha = alpha * jnp.exp(before)
    start_recept = recept_b * jnp.exp(falling)
    drop = jnp.exp(ending - falling)
    end_beta = beta * drop
    end_keys = written_b * drop
    end_decay = jnp.exp(ending)[:, :, 0, :]
    identity = jnp.broadcast_to(jnp.eye(HEAD_SIZE, dtype=jnp.float32), (segments, HEAD_SIZE, HEAD_SIZE))
    state = jnp.concatenate([jnp.zeros_like(identity), identity], axis=-1)
    reads = []
    for n in range(steps):
        rows = jnp.einsum("qfl,qlz->qfz", start_alpha[n], state, precision=exact_setting) + rhs_local[n]
        removed = jnp.einsum("hti,hiv->htv", inverse[n], rows, precision=exact_setting)
        reads.append(
            jnp.einsum("qfl,qlz->qfz", start_recept[n], state, precision=exact_setting)
            + jnp.einsum("hti,hiv->htv", recept_beta[n], removed, precision=exact_setting)
            + read_local[n]
        )
        state = (
            end_decay[n][:, :, None] * state
            + jnp.einsum("pzw,pzb->pwb", end_beta[n], removed, precision=exact_setting)
            + jnp.einsum("pzw,pzb->pwb", end_keys[n], widened[n], precision=exact_setting)
        )
    reads = jnp.stack(reads, axis=1).reshape(segments, SEGMENT, 2 * HEAD_SIZE)
    return reads, state


def matmul(left, right):
    return jnp.dot(left, right, precision=exact_setting)


def shards(
    tokens, norm_gain, query_weight, key_weight, value_weight, decay_weight, removal_weight, gate_weight,
    key_gain, removal_gain, removal_bias, decay_bias, decay_extra, scan_norm_gain,
    conv_value_weight, conv_gate_weight, conv_kernel, conv_bias, conv_norm_gain,
    out_scan_weight, out_conv_weight,
):
    nsp, ntp = lax.axis_size("sp"), lax.axis_size("tp")
    s = lax.axis_index("sp")
    p, y = s // 2, s % 2
    npair = nsp // 2
    group = nsp // ntp
    rows = tokens.shape[0]
    length = 2 * rows
    matrices = (
        query_weight, key_weight, value_weight, decay_weight,
        removal_weight, gate_weight, conv_value_weight, conv_gate_weight,
    )
    halves = jnp.stack(
        [
            jnp.concatenate([m[:, h * HEAD_SIZE : (h + 1) * HEAD_SIZE] for m in matrices], axis=1)
            for h in range(2)
        ]
    )
    extra = jnp.stack([decay_extra[:, :HEAD_SIZE], decay_extra[:, HEAD_SIZE:]])
    outw = jnp.concatenate(
        [w[h * HEAD_SIZE : (h + 1) * HEAD_SIZE] for h in range(2) for w in (out_scan_weight, out_conv_weight)],
        axis=0,
    )
    depth, columns = halves.shape[1:]
    model = depth * nsp
    dma = pltpu.SemaphoreType.DMA
    proj, extra_all, outw_all = call(
        functools.partial(project_kernel, nsp, ntp),
        (
            jax.ShapeDtypeStruct((length + HALO, columns), jnp.bfloat16),
            jax.ShapeDtypeStruct((2, rows, HEAD_SIZE), jnp.float32),
            jax.ShapeDtypeStruct((group, ntp) + outw.shape, jnp.bfloat16),
        ),
        [
            pltpu.VMEM((ntp, length + HALO, tokens.shape[1]), jnp.bfloat16),
            pltpu.VMEM((length + HALO, model), jnp.bfloat16),
            pltpu.VMEM((model, columns), jnp.bfloat16),
            dma((1,)), dma((nsp,)), dma((nsp,)), dma((nsp,)),
            dma((2 * ntp,)), dma((2 * ntp,)), dma((2 * ntp,)), dma((ntp,)),
            dma((npair,)), dma((group * ntp,)), dma((group * ntp,)), dma((1,)), dma((1,)), dma((3,)),
        ],
        tokens, norm_gain.reshape(1, model), halves, extra, outw,
    )

    def half_of(a):
        return lax.dynamic_slice_in_dim(a, y * HEAD_SIZE, HEAD_SIZE, a.ndim - 1)

    floats = proj.astype(jnp.float32)
    pieces = [floats[:, i * HEAD_SIZE : (i + 1) * HEAD_SIZE] for i in range(len(matrices))]
    recept, key_rows, values, decay_pre, removal_pre, gate_pre = [a[HALO:] for a in pieces[:6]]
    reads, segment_state = local_scan(
        recept, key_rows, values, decay_pre, removal_pre,
        half_of(key_gain), half_of(removal_gain), half_of(removal_bias), half_of(decay_bias),
        extra_all.reshape(length, HEAD_SIZE),
    )
    segments = segment_state.shape[0]
    prefix = []
    total = None
    for j in range(segments):
        prefix.append(total)
        local = segment_state[j]
        if total is None:
            total = local
        else:
            moved = matmul(local[:, HEAD_SIZE:], total)
            total = moved + jnp.concatenate([local[:, :HEAD_SIZE], jnp.zeros_like(local[:, :HEAD_SIZE])], axis=1)

    padded = (pieces[6] * jax.nn.sigmoid(pieces[7])).astype(jnp.bfloat16).astype(jnp.float32)
    taps = half_of(conv_kernel)
    first = HALO - (CONV_K - 1)
    filtered = half_of(conv_bias) + taps[0] * padded[first : first + length]
    for index in range(1, CONV_K):
        filtered = filtered + taps[index] * padded[first + index : first + index + length]
    stats = jnp.stack([jnp.sum(filtered, axis=-1), jnp.sum(filtered * filtered, axis=-1)])

    states, stats_all = call(
        functools.partial(state_kernel, nsp, ntp),
        (
            jax.ShapeDtypeStruct((npair,) + total.shape, jnp.float32),
            jax.ShapeDtypeStruct((2 * ntp,) + stats.shape, jnp.float32),
        ),
        [dma((npair,)), dma((npair,)), dma((2 * ntp,)), dma((2 * ntp,)), dma((1,))],
        total, stats,
    )

    def step(k, incoming):
        item = lax.dynamic_index_in_dim(states, k, 0, False)
        moved = matmul(item[:, HEAD_SIZE:], incoming) + item[:, :HEAD_SIZE]
        return jnp.where(k < p, moved, incoming)

    incoming = jnp.zeros((HEAD_SIZE, HEAD_SIZE), jnp.float32)
    for k in range(npair - 1) if npair <= 8 else ():
        incoming = step(k, incoming)
    if npair > 8:
        incoming = lax.fori_loop(0, npair - 1, step, incoming)
    starts = []
    for j in range(segments):
        if prefix[j] is None:
            starts.append(incoming)
        else:
            starts.append(matmul(prefix[j][:, HEAD_SIZE:], incoming) + prefix[j][:, :HEAD_SIZE])
    read = reads[..., :HEAD_SIZE] + jnp.einsum(
        "yem,ymb->yeb", reads[..., HEAD_SIZE:], jnp.stack(starts), precision=exact_setting
    )
    read = read.reshape(length, HEAD_SIZE)
    center = jnp.mean(read, axis=-1, keepdims=True)
    spread = jnp.mean((read - center) ** 2, axis=-1, keepdims=True)
    scan_out = (
        (read - center) * lax.rsqrt(spread + 0.00064) * half_of(scan_norm_gain) * jax.nn.sigmoid(gate_pre)
    ).astype(jnp.bfloat16)

    totals = jnp.sum(stats_all, axis=0)
    channels = 2 * ntp * HEAD_SIZE
    center = totals[0] / channels
    spread = totals[1] / channels - center * center
    scaled = (filtered - center[:, None]) * lax.rsqrt(spread[:, None] + 1e-05) * half_of(conv_norm_gain)
    conv_out = jax.nn.silu(scaled).astype(jnp.bfloat16)
    features = jnp.concatenate([scan_out, conv_out], axis=1).reshape(2, rows, 2 * HEAD_SIZE)
    gathered = call(
        functools.partial(feature_kernel, ntp),
        jax.ShapeDtypeStruct((rows, 4 * ntp * HEAD_SIZE), jnp.bfloat16),
        [dma((2 * ntp,)), dma((2 * ntp,)), dma((1,))],
        features,
    )
    regrouped = outw_all.transpose(1, 2, 0, 3).reshape(gathered.shape[1], -1)
    return jnp.dot(gathered, regrouped, preferred_element_type=jnp.float32).astype(jnp.bfloat16)


def solution(mesh):
    two = P("sp", "tp")
    one = P("tp")
    placed = (
        two, P(), two, two, two, two, two, two, one, one, one, one, two, one,
        two, two, P(None, "tp"), one, one, P("tp", "sp"), P("tp", "sp"),
    )
    return jax.shard_map(shards, mesh=mesh, in_specs=placed, out_specs=two, check_vma=False)
```

time: 396 us -> 143 us (0.36)
  blocking collectives: 348 us -> 0 us
  Pallas kernels: 0 us -> 97.5 us
  local copies, waits for them, and re-layouts: 5.31 us -> 21.3 us
  between operations: 14 us -> 0.83 us
  starting transfers between devices: 7.14 us -> 0 us
    all_gather x12 -> x0, blocking collectives: 333 us -> none  [the longest x2 62.3 us: carried_in(): gathered = jax.tree.map(lambda a: lax.all_gather(a, axis), part)]
    pallas_call x0 -> x3, Pallas kernels: none -> 97.5 us  [call(): pl.pallas_call(kernel, out_shape=outs, in_specs=[vmem] * len(operands), o...]
    psum x1 -> x0, blocking collectives: 15.4 us -> none  [conv_mixer(): lax.psum((jnp.sum(filtered, axis=-1), jnp.sum(filtered * filtered, axis=-...]
    unnamed x40 -> x88, local copies, waits for them, and re-layouts: 2.73 us -> 15.3 us
    dot_general x46 -> x30, matrix products: 12.8 us -> 14 us  [the longest x9 6.96 us: matmul(): return jnp.dot(left, right, precision=exact_setting)]
  transfers between devices with their start and end apart: 3 -> 0, of which waited for: 0 -> 0; matrix products, arithmetic and copies ran while one was open for 5% -> 0% of each run, Pallas kernels for 0% -> 0%
where the time goes in v1:
time: 143 us; the launch traced here: 142 us
  Pallas kernels  97.5 us (68%)
  local copies, waits for them, and re-layouts  21.3 us (15%)
  matrix products  19 us (13%)
  other arithmetic  3.12 us (2%)
    pallas_call x3, Pallas kernels, call(): pl.pallas_call(kernel, out_shape=outs, in_specs=[vmem] * len(operands), o...  97.5 us
    unnamed x88, local copies, waits for them, and re-layouts  15.3 us
    dot_general x9, matrix products, matmul(): return jnp.dot(left, right, precision=exact_setting)  6.96 us
    dot_general x10, matrix products, block_product(): return jnp.einsum('nhij,nhjk->nhik', left, right, precision=exact_setting)  3.18 us

profile of v1, /device:TPU:0, one launch (start us, length us, event | category | flops | bytes accessed | tf_op | source)
XLA Modules:
  0.0 141.8 jit_solution(3611332596587379276)
XLA Ops:
  0.0 0.7 copy-done.36
  0.7 1.1 fusion.128
  2.0 0.7 copy-done.16
  2.8 0.7 copy-done.18
  4.2 0.8 copy-done.24
  5.0 0.9 copy-done.9
  6.1 0.9 copy-done
  6.9 75.8 %shard_map.199 = (bf16[416,512]{1,0:T(8,128)(2,1)S(1)}, f32[2,192,64]{2,1,0:T(8,128)S(1)}, bf16[2,4,256,256]{3,2,1,0:T(8,128)(2,1)S(1)}) custom-call(bf16[192,512]{1,0:T(8,128)(2,1)S(1)} %copy-done, f32[1,2048]{1,0:T(1,128)S(1)} %bitcast.293, bf16[2,256,512]{2,1,0:T(8,128)(2,1)S(1)} %pad_maximum_fusion.weights, f32[2,192,64]{2,1,0:T(8,128)S(1)} %pad_maximum_fusion.1.extra, ...), custom_call_target="tpu_custom_call" | custom-call | tf_op jit(solution)/shard_map/pallas_call | solution.py:330
  83.1 0.6 copy-done.37
  83.8 0.6 copy-done.38
  84.5 0.6 copy-done.39
  85.1 0.3 multiply_multiply_fusion
  85.7 0.9 bitcast_multiply_fusion
  86.6 0.5 convolution_multiply_fusion.2
  87.0 0.3 fusion.138
  87.4 0.3 convolution_add_fusion.3
  87.7 0.3 fusion.139
  88.0 0.3 convolution_add_fusion.2
  88.3 0.3 fusion.140
  88.7 0.3 convolution_add_fusion.1
  89.0 0.3 fusion.141
  89.3 0.3 convolution_add_fusion
  89.6 0.5 convolution_multiply_fusion.1
  90.1 0.3 fusion.74
  90.5 0.3 convolution_add_fusion.16
  91.0 0.4 convolution_add_fusion.9
  91.6 0.4 convolution_add_fusion.8
  92.5 0.4 convolution_add_fusion.7
  93.1 0.4 convolution_add_fusion.6
  93.9 0.6 copy-done.7
  94.5 0.4 convolution_add_fusion.5
  95.0 0.4 convolution_add_fusion.4
  95.4 0.6 slice_bitcast_fusion.44
  96.0 0.7 copy-done.27
  97.1 0.4 copy-done.10
  97.7 0.4 copy-done.12
  98.1 0.7 copy-done.26
  98.8 0.7 dynamic-slice_bitcast_fusion.30
  99.6 0.7 copy-done.40
  100.5 0.5 copy-done.28
  101.0 0.8 fusion.123
  101.9 9.3 %shard_map.200 = (f32[4,64,128]{2,1,0:T(8,128)S(1)}, f32[8,2,384]{2,1,0:T(2,128)S(1)}) custom-call(f32[64,128]{1,0:T(8,128)S(1)} %convolution_add_fusion.23.state, f32[2,384]{1,0:T(2,128)S(1)} %pad_maximum_fusion.5.stats), custom_call_target="tpu_custom_call" | custom-call | tf_op jit(solution)/shard_map/pallas_call | solution.py:330
  111.1 0.7 slice_bitcast_fusion.50
  111.8 1.1 fusion.12
  112.9 1.7 %fusion.11 = f32[64,64]{1,0:T(8,128)} fusion(f32[64,64]{1,0:T(8,128)S(1)} %fusion.12, f32[64,128]{1,0:T(8,128)} %get-tuple-element.43, pred[]{:T(512)S(6)} %gt.26), kind=kOutput, calls=%fused_computation.39 | convolution fusion | flops 3153920 | bytes 147457 | tf_op jit(solution)/shard_map/dot_general | solution.py:424
  114.5 1.1 fusion.10
  115.6 0.8 fusion.9
  116.5 0.8 fusion.8
  117.3 0.8 fusion.7
  118.1 0.5 convolution_multiply_fusion.3
  118.6 0.5 convolution_multiply_fusion
  119.1 0.3 fusion.72
  119.4 0.6 copy-done.2
  120.0 0.3 fusion.14
  120.4 0.5 copy-done.4
  121.3 0.6 copy-done.6
  122.4 0.6 copy-done.8
  123.3 0.6 copy-done.20
  124.0 0.6 fusion.137
  125.0 0.6 copy-done.41
  125.9 0.6 copy-done.42
  126.9 12.5 %shard_map.201 = bf16[192,1024]{1,0:T(8,128)(2,1)S(1)} custom-call(bf16[2,192,128]{2,1,0:T(8,128)(2,1)S(1)} %bitcast.292), custom_call_target="tpu_custom_call" | custom-call | tf_op jit(solution)/shard_map/pallas_call | solution.py:330
  139.4 1.1 copy.41
  140.8 1.1 convolution_convert_fusion
  (127 shorter events, 7.0 us)
Async XLA Ops:
  0.0 0.7 copy-start.36
  0.7 1.1 copy-start.14
  0.7 1.1 copy-start.15
  1.8 0.8 copy-start.16
  1.8 0.9 copy-start.17
  2.7 0.8 copy-start.18
  2.7 0.9 copy-start.19
  4.1 0.8 copy-start.24
  4.1 0.9 copy-start.25
  5.0 0.9 copy-start.9
  6.0 0.9 copy-start
  6.0 0.9 copy-start.1
  83.1 0.7 copy-start.37
  83.7 0.7 copy-start.38
  84.4 0.7 copy-start.39
  91.0 0.6 copy-start.3
  92.5 0.6 copy-start.5
  93.9 0.6 copy-start.7
  96.0 0.7 copy-start.27
  96.9 0.6 copy-start.10
  97.5 0.6 copy-start.12
  98.1 0.7 copy-start.26
  99.6 0.7 copy-start.40
  100.3 0.7 copy-start.28
  100.3 0.7 copy-start.29
  100.3 0.7 copy-start.30
  100.3 0.7 copy-start.31
  100.3 0.7 copy-start.32
  100.3 0.7 copy-start.33
  100.3 0.7 copy-start.34
  100.4 0.7 copy-start.35
  114.5 1.1 copy-start.23
  115.6 0.8 copy-start.11
  116.4 0.8 copy-start.13
  119.1 0.9 copy-start.2
  120.0 0.8 copy-start.4
  121.1 0.8 copy-start.6
  122.1 0.8 copy-start.8
  123.2 0.8 copy-start.20
  123.2 0.8 copy-start.21
  123.2 0.8 copy-start.22
  124.9 0.7 copy-start.41
  125.9 0.7 copy-start.42

commit v2 on v1

v2 whole, which is shorter than its diff:
```python
import functools

import jax
import jax.numpy as jnp
from jax import lax
from jax.experimental import pallas as pl
from jax.experimental.pallas import tpu as pltpu
from jax.sharding import PartitionSpec as P

HEAD_SIZE = 64
CONV_K = 31
HALO = 32
BLOCK = 64
MESH = pl.DeviceIdType.MESH


def remote(src, dst, send, recv, sp, tp):
    return pltpu.make_async_remote_copy(
        src_ref=src, dst_ref=dst, send_sem=send, recv_sem=recv,
        device_id={"sp": sp, "tp": tp}, device_id_type=MESH,
    )


def project_kernel(
    nsp, ntp, tokens, gain, weights, extra,
    proj, extra_all,
    tok, normed, full,
    send_y, recv_w, send_up, send_dn, send_tok, recv_tok, send_halo, recv_halo,
    send_ex, recv_ex, local,
):
    s, t = lax.axis_index("sp"), lax.axis_index("tp")
    p, y = s // 2, s % 2
    np_ = nsp // 2
    mate = 2 * p + 1 - y
    rows = tokens.shape[0]
    depth = weights.shape[1]

    def slot(b):
        return full.at[pl.ds(pl.multiple_of(b * depth, depth), depth), :]

    def place(yy, q):
        return tok.at[q, pl.ds(pl.multiple_of(HALO + yy * rows, 16), rows), :]

    def weight_copy(b, yy, sems, to):
        i = 2 * b + yy
        return remote(slot(i), slot(i), sems.at[i], recv_w.at[i], 2 * to + y, t)

    own = pltpu.make_async_copy(weights.at[y], slot(s), local.at[0])
    own.start()
    swap = remote(weights.at[1 - y], slot(s), send_y.at[0], recv_w.at[s], mate, t)
    swap.start()

    def send_own(sems, to):
        return remote(weights.at[y], slot(s), sems.at[s], recv_w.at[s], 2 * to + y, t)

    @pl.when(p + 1 < np_)
    def _():
        send_own(send_up, p + 1).start()

    @pl.when(p > 0)
    def _():
        send_own(send_dn, p - 1).start()

    mine = pltpu.make_async_copy(tokens, place(y, t), local.at[1])
    mine.start()
    group_size = 2 * ntp
    me = y * ntp + t

    def tok_send(d):
        g = lax.rem(me + d, group_size)
        return remote(tokens, place(y, t), send_tok.at[d], recv_tok.at[me], 2 * p + g // ntp, g % ntp)

    def halo_send(g):
        return remote(
            tokens.at[pl.ds(rows - HALO, HALO), :], tok.at[t, pl.ds(0, HALO), :],
            send_halo.at[g], recv_halo.at[t], 2 * (p + 1) + g // ntp, g % ntp,
        )

    for d in range(1, group_size):
        tok_send(d).start()
    sends_halo = jnp.logical_and(y == 1, p + 1 < np_)

    @pl.when(sends_halo)
    def _():
        for g in range(group_size):
            halo_send(g).start()

    ex_own = pltpu.make_async_copy(extra.at[y], extra_all.at[y], local.at[2])
    ex_own.start()
    ex = remote(extra.at[1 - y], extra_all.at[y], send_ex.at[0], recv_ex.at[0], mate, t)
    ex.start()

    own.wait()
    remote(slot(mate), slot(mate), send_y.at[0], recv_w.at[mate], mate, t).wait_recv()

    @pl.when(p + 1 < np_)
    def _():
        weight_copy(p, 1 - y, send_up, p + 1).start()

    @pl.when(p > 0)
    def _():
        weight_copy(p, 1 - y, send_dn, p - 1).start()

    def line(k, c):
        for e in range(2):
            yy = lax.rem(y + e, 2)
            low, high = p - k, p + k

            @pl.when(low >= 0)
            def _():
                weight_copy(low, yy, send_up, p).wait_recv()

                @pl.when(p + 1 < np_)
                def _():
                    weight_copy(low, yy, send_up, p + 1).start()

            @pl.when(high < np_)
            def _():
                weight_copy(high, yy, send_dn, p).wait_recv()

                @pl.when(p > 0)
                def _():
                    weight_copy(high, yy, send_dn, p - 1).start()

        return c

    lax.fori_loop(1, 2, line, 0)

    mine.wait()
    for d in range(1, group_size):
        g = lax.rem(me + d, group_size)
        view = place(g // ntp, g % ntp)
        remote(view, view, send_tok.at[0], recv_tok.at[g], mate, t).wait_recv()

    @pl.when(p > 0)
    def _():
        for q in range(ntp):
            view = tok.at[q, pl.ds(0, HALO), :]
            remote(view, view, send_tok.at[0], recv_halo.at[q], mate, t).wait_recv()

    @pl.when(p == 0)
    def _():
        tok[:, 0:HALO, :] = jnp.zeros((ntp, HALO, tok.shape[2]), tok.dtype)

    width = tok.shape[2]
    total_rows = tok.shape[1]
    tile = HALO

    def norm_tile(i, c):
        at = pl.ds(pl.multiple_of(i * tile, tile), tile)
        squares = jnp.zeros((tile, 1), jnp.float32)
        for q in range(ntp):
            x = tok[q, at, :].astype(jnp.float32)
            squares = squares + jnp.sum(x * x, axis=-1, keepdims=True)
        scale = lax.rsqrt(squares / (ntp * width) + 1e-06)
        for q in range(ntp):
            x = tok[q, at, :].astype(jnp.float32)
            g = gain[:, q * width : (q + 1) * width]
            normed[at, q * width : (q + 1) * width] = (x * scale * g).astype(jnp.bfloat16)
        return c

    lax.fori_loop(0, total_rows // tile, norm_tile, 0)
    lax.fori_loop(2, np_, line, 0)

    columns = full.shape[1]
    for n in range(0, columns, 256):
        proj[:, n : n + 256] = jnp.dot(
            normed[...], full[:, n : n + 256], preferred_element_type=jnp.float32
        ).astype(jnp.bfloat16)

    swap.wait_send()
    ex_own.wait()
    ex.wait()
    for d in range(1, group_size):
        tok_send(d).wait_send()

    @pl.when(sends_halo)
    def _():
        for g in range(group_size):
            halo_send(g).wait_send()

    def end_out(k, c):
        for yy in range(2):

            @pl.when(jnp.logical_and(k <= p, p + 1 < np_))
            def _():
                weight_copy(k, yy, send_up, p).wait_send()

            @pl.when(jnp.logical_and(k >= p, p > 0))
            def _():
                weight_copy(k, yy, send_dn, p).wait_send()

        return c

    lax.fori_loop(0, np_, end_out, 0)


def dot(left, right, contract=(1, 0)):
    def one(a, b):
        return lax.dot_general(
            a, b, (((contract[0],), (contract[1],)), ((), ())), preferred_element_type=jnp.float32
        )

    left_high, right_high = left.astype(jnp.bfloat16), right.astype(jnp.bfloat16)
    left_low = (left - left_high.astype(jnp.float32)).astype(jnp.bfloat16)
    right_low = (right - right_high.astype(jnp.float32)).astype(jnp.bfloat16)
    return one(left_high, right_high) + (one(left_high, right_low) + one(left_low, right_high))


def sigmoid(x):
    return 1.0 / (1.0 + jnp.exp(-x))


def mixer_kernel(
    nsp, ntp, proj, extra, key_gain, removal_gain, removal_bias, decay_bias, scan_gain,
    conv_bias, conv_gain, taps, outw,
    out,
    outw_all, reads, total_ref, states, padded, filt, stats, stats_all, features, gathered, prefix, arriving,
    send_out, recv_out, send_fwd, send_st, recv_st, send_g, recv_g, send_f, recv_f, local,
):
    s, t = lax.axis_index("sp"), lax.axis_index("tp")
    p, y = s // 2, s % 2
    np_ = nsp // 2
    mate = 2 * p + 1 - y
    group = nsp // ntp
    half = group // 2
    group_size = 2 * ntp
    length = 2 * extra.shape[1]
    rows = extra.shape[1]
    size = HEAD_SIZE

    j, q_to = s % group, s // group
    y_to = j // half

    def out_send(k):
        return remote(
            outw, outw_all.at[j, t], send_out.at[k], recv_out.at[j * ntp + t], 2 * k + y_to, q_to
        )

    def is_self(k):
        return jnp.logical_and(2 * k + y_to == s, q_to == t)

    def start_out(k, c):
        @pl.when(is_self(k))
        def _():
            pltpu.make_async_copy(outw, outw_all.at[j, t], recv_out.at[j * ntp + t]).start()

        @pl.when(jnp.logical_not(is_self(k)))
        def _():
            out_send(k).start()

        return c

    lax.fori_loop(0, np_, start_out, 0)

    def mine(ref):
        whole = ref[...]
        return jnp.where(y == 0, whole[:, :size], whole[:, size:])

    k_gain, r_gain, r_bias, d_bias = mine(key_gain), mine(removal_gain), mine(removal_bias), mine(decay_bias)

    def column(i, start, count):
        pair = proj[start : start + count, (i // 2) * 2 * size : (i // 2 + 1) * 2 * size]
        return pair[:, (i % 2) * size : (i % 2 + 1) * size].astype(jnp.float32)

    side = 2 * BLOCK
    row = lax.broadcasted_iota(jnp.int32, (side, side), 0)
    col = lax.broadcasted_iota(jnp.int32, (side, side), 1)
    same = row // BLOCK == col // BLOCK
    strict = jnp.logical_and(same, row > col)
    inclusive = jnp.logical_and(same, row >= col)
    same16 = row // 16 == col // 16
    same32 = row // 32 == col // 32
    tri = jnp.where(inclusive, 1.0, 0.0)
    unit = jnp.where(row == col, 1.0, 0.0)
    eye = unit[:size, :size]
    maps = []
    for n in range(length // side):
        at = n * side
        recept, keys, values, decay_pre, removal_pre = [column(i, HALO + at, side) for i in range(5)]
        member, begin = divmod(at, rows)
        if begin + side <= rows:
            more = extra[member, begin : begin + side, :]
        else:
            more = jnp.concatenate([extra[member, begin:rows, :], extra[member + 1, 0 : begin + side - rows, :]], axis=0)
        rate = sigmoid(d_bias + decay_pre) * jnp.exp(jnp.float32(-0.5)) + more
        removal = sigmoid(r_bias + removal_pre)
        scaled = keys * k_gain
        unit_keys = scaled * lax.rsqrt(jnp.sum(scaled * scaled, axis=-1, keepdims=True) + 1e-06)
        written = keys * (1.0 + (removal - 1.0) * r_gain)
        falling = -dot(tri, rate)
        before = falling + rate

        def spread_row(offset):
            return jnp.concatenate(
                [
                    jnp.broadcast_to(falling[b * BLOCK + offset : b * BLOCK + offset + 1, :], (BLOCK, size))
                    for b in range(2)
                ],
                axis=0,
            )

        middle, ending = spread_row(BLOCK // 2), spread_row(BLOCK - 1)
        alpha = -unit_keys
        beta = unit_keys * removal
        lift = jnp.exp(middle - falling)
        left = jnp.concatenate([alpha * jnp.exp(before - middle), recept * jnp.exp(falling - middle)], axis=0)
        right = jnp.concatenate([beta * lift, written * lift], axis=0)
        prod = dot(left, right, (1, 1))
        alpha_beta = jnp.where(strict, prod[:side, :side], 0.0)
        alpha_keys = jnp.where(strict, prod[:side, side:], 0.0)
        recept_beta = jnp.where(inclusive, prod[side:, :side], 0.0)
        recept_keys = jnp.where(inclusive, prod[side:, side:], 0.0)
        power = jnp.where(same16, alpha_beta, 0.0)
        solve = unit + power
        for _ in range(3):
            power = dot(power, power)
            solve = solve + dot(solve, power)
        for edge in (
            jnp.where(jnp.logical_and(same32, jnp.logical_not(same16)), alpha_beta, 0.0),
            jnp.where(same32, 0.0, alpha_beta),
        ):
            solve = solve + dot(solve, dot(edge, solve))
        both = dot(jnp.concatenate([alpha_keys, recept_keys], axis=0), values)
        removed = dot(solve, jnp.concatenate([both[:side], alpha * jnp.exp(before)], axis=1))
        reads[at : at + side, :] = jnp.concatenate(
            [both[side:], recept * jnp.exp(falling)], axis=1
        ) + dot(recept_beta, removed)
        drop = jnp.exp(ending - falling)
        end_beta, end_keys = beta * drop, written * drop
        for b in range(2):
            part = slice(b * BLOCK, (b + 1) * BLOCK)
            last = falling[(b + 1) * BLOCK - 1 : (b + 1) * BLOCK, :]
            maps.append(
                jnp.concatenate([dot(end_keys[part].T, values[part]), eye * jnp.exp(last)], axis=1)
                + dot(end_beta[part].T, removed[part])
            )

    total = None
    for n, local_map in enumerate(maps):
        prefix[n] = jnp.concatenate([jnp.zeros((size, size), jnp.float32), eye], axis=1) if total is None else total
        if total is None:
            total = local_map
        else:
            total = dot(local_map[:, size:], total) + jnp.concatenate(
                [local_map[:, :size], jnp.zeros((size, size), jnp.float32)], axis=1
            )
    total_ref[...] = total

    padded[...] = (
        (column(6, 0, length + HALO) * sigmoid(column(7, 0, length + HALO))).astype(jnp.bfloat16).astype(jnp.float32)
    )
    tap = mine(taps)
    first = HALO - (CONV_K - 1)
    bias = mine(conv_bias)
    ones = jnp.ones((8, size), jnp.float32)
    for n in range(length // side):
        at = n * side
        filtered = bias + tap[0:1] * padded[first + at : first + at + side, :]
        for i in range(1, CONV_K):
            filtered = filtered + tap[i : i + 1] * padded[first + i + at : first + i + at + side, :]
        filt[at : at + side, :] = filtered
        stats[0:8, at : at + side] = dot(ones, filtered, (1, 1))
        stats[8:16, at : at + side] = dot(ones, filtered * filtered, (1, 1))

    def st(k):
        return remote(total_ref, states.at[p], send_st.at[k], recv_st.at[p], 2 * k + y, t)

    def start_state(k, c):
        st(k).start()
        return c

    lax.fori_loop(p + 1, np_, start_state, 0)
    me = 2 * t + y

    def send_stats(d):
        g = lax.rem(me + d, group_size)
        return remote(stats, stats_all.at[me], send_g.at[d], recv_g.at[me], 2 * p + g % 2, g // 2)

    for d in range(1, group_size):
        send_stats(d).start()

    def out_view(i):
        return outw_all.at[i // ntp, i % ntp]

    def forward(i):
        return remote(out_view(i), out_view(i), send_fwd.at[i], recv_out.at[i], mate, t)

    base = y * half * ntp
    other = (1 - y) * half * ntp

    def start_forward(i, c):
        forward(base + i).wait_recv()
        forward(base + i).start()
        return c

    lax.fori_loop(0, half * ntp, start_forward, 0)

    def arrived(k, c):
        remote(states.at[k], states.at[k], send_st.at[k], recv_st.at[k], 2 * k + y, t).wait_recv()
        return c

    lax.fori_loop(0, p, arrived, 0)
    still = jnp.concatenate([jnp.zeros((size, size), jnp.float32), eye], axis=1)
    incoming = jnp.zeros((size, size), jnp.float32)
    for k in range(np_ - 1):
        item = jnp.where(k < p, states[k], still)
        incoming = dot(item[:, size:], incoming) + item[:, :size]
    gain = mine(scan_gain)
    arriving[0] = incoming

    def finish(n, c):
        at = pl.ds(pl.multiple_of(n * BLOCK, BLOCK), BLOCK)
        begin = dot(prefix[n, :, size:], arriving[n // np_count]) + prefix[n, :, :size]
        block = reads[at, :]
        read = block[:, :size] + dot(block[:, size:], begin)
        center = jnp.mean(read, axis=-1, keepdims=True)
        spread = jnp.mean((read - center) ** 2, axis=-1, keepdims=True)
        gate_at = pl.ds(pl.multiple_of(HALO + n * BLOCK, HALO), BLOCK)
        gate = sigmoid(proj[gate_at, 4 * size : 6 * size].astype(jnp.float32)[:, size:])
        features[at, 0:size] = (
            (read - center) * lax.rsqrt(spread + 0.00064) * gain * gate
        ).astype(jnp.bfloat16)
        return c

    np_count = length // BLOCK
    lax.fori_loop(0, np_count, finish, 0)
    totals = stats[...]
    for d in range(1, group_size):
        g = lax.rem(me + d, group_size)
        remote(stats_all.at[g], stats_all.at[g], send_g.at[d], recv_g.at[g], s, t).wait_recv()
        totals = totals + stats_all[g]
    totals = totals / (group_size * size)
    center = totals[0:8]
    inverse = lax.rsqrt(totals[8:16] - center * center + 1e-05)
    center, inverse = center.T, inverse.T
    scaled = (filt[...] - center[:, 0:1]) * inverse[:, 0:1] * mine(conv_gain)
    features[:, size:] = (scaled * sigmoid(scaled)).astype(jnp.bfloat16)

    def end_forward(i, c):
        forward(other + i).wait_recv()
        forward(base + i).wait_send()
        return c

    wide = 2 * size

    def columns(g):
        return gathered.at[:, pl.ds(pl.multiple_of(g * wide, 128), wide)]

    def part_of(yy):
        return features.at[pl.ds(pl.multiple_of(yy * rows, 16), rows), :]

    def send(d):
        g = lax.rem(me + d, group_size)
        return remote(part_of(g % 2), columns(me), send_f.at[d], recv_f.at[me], 2 * p + g % 2, g // 2)

    for d in range(1, group_size):
        send(d).start()
    copy = pltpu.make_async_copy(part_of(y), columns(me), local.at[0])
    copy.start()

    lax.fori_loop(0, half * ntp, end_forward, 0)

    def end_out(k, c):
        @pl.when(jnp.logical_not(is_self(k)))
        def _():
            out_send(k).wait_send()

        return c

    lax.fori_loop(0, np_, end_out, 0)

    def end_state(k, c):
        st(k).wait_send()
        return c

    lax.fori_loop(p + 1, np_, end_state, 0)
    for d in range(1, group_size):
        send_stats(d).wait_send()
    for d in range(1, group_size):
        g = lax.rem(me + d, group_size)
        remote(columns(g), columns(g), send_f.at[d], recv_f.at[g], s, t).wait_recv()
        send(d).wait_send()
    copy.wait()
    strip = outw.shape[1]
    for i in range(group):
        weight = outw_all[i].reshape(gathered.shape[1], strip)
        out[:, i * strip : (i + 1) * strip] = jnp.dot(
            gathered[...], weight, preferred_element_type=jnp.float32
        ).astype(jnp.bfloat16)


def call(kernel, outs, scratch, *operands):
    vmem = pl.BlockSpec(memory_space=pltpu.VMEM)
    return pl.pallas_call(
        kernel,
        out_shape=outs,
        in_specs=[vmem] * len(operands),
        out_specs=jax.tree.map(lambda _: vmem, outs),
        scratch_shapes=scratch,
        compiler_params=pltpu.CompilerParams(
            has_side_effects=True, vmem_limit_bytes=40 * 1024 * 1024
        ),
    )(*operands)


def shards(
    tokens, norm_gain, query_weight, key_weight, value_weight, decay_weight, removal_weight, gate_weight,
    key_gain, removal_gain, removal_bias, decay_bias, decay_extra, scan_norm_gain,
    conv_value_weight, conv_gate_weight, conv_kernel, conv_bias, conv_norm_gain,
    out_scan_weight, out_conv_weight,
):
    nsp, ntp = lax.axis_size("sp"), lax.axis_size("tp")
    npair = nsp // 2
    group = nsp // ntp
    rows = tokens.shape[0]
    length = 2 * rows
    matrices = (
        query_weight, key_weight, value_weight, decay_weight,
        removal_weight, gate_weight, conv_value_weight, conv_gate_weight,
    )
    halves = jnp.stack(
        [
            jnp.concatenate([m[:, h * HEAD_SIZE : (h + 1) * HEAD_SIZE] for m in matrices], axis=1)
            for h in range(2)
        ]
    )
    extra = jnp.stack([decay_extra[:, :HEAD_SIZE], decay_extra[:, HEAD_SIZE:]])
    outw = jnp.concatenate(
        [w[h * HEAD_SIZE : (h + 1) * HEAD_SIZE] for h in range(2) for w in (out_scan_weight, out_conv_weight)],
        axis=0,
    )
    depth, columns = halves.shape[1:]
    model = depth * nsp
    dma = pltpu.SemaphoreType.DMA
    proj, extra_all = call(
        functools.partial(project_kernel, nsp, ntp),
        (
            jax.ShapeDtypeStruct((length + HALO, columns), jnp.bfloat16),
            jax.ShapeDtypeStruct((2, rows, HEAD_SIZE), jnp.float32),
        ),
        [
            pltpu.VMEM((ntp, length + HALO, tokens.shape[1]), jnp.bfloat16),
            pltpu.VMEM((length + HALO, model), jnp.bfloat16),
            pltpu.VMEM((model, columns), jnp.bfloat16),
            dma((1,)), dma((nsp,)), dma((nsp,)), dma((nsp,)),
            dma((2 * ntp,)), dma((2 * ntp,)), dma((2 * ntp,)), dma((ntp,)),
            dma((1,)), dma((1,)), dma((3,)),
        ],
        tokens, norm_gain.reshape(1, model), halves, extra,
    )
    bf, f32 = jnp.bfloat16, jnp.float32
    group_size = 2 * ntp
    return call(
        functools.partial(mixer_kernel, nsp, ntp),
        jax.ShapeDtypeStruct((rows, group * outw.shape[1]), bf),
        [
            pltpu.VMEM((group, ntp) + outw.shape, bf),
            pltpu.VMEM((length, 2 * HEAD_SIZE), f32),
            pltpu.VMEM((HEAD_SIZE, 2 * HEAD_SIZE), f32),
            pltpu.VMEM((npair, HEAD_SIZE, 2 * HEAD_SIZE), f32),
            pltpu.VMEM((length + HALO, HEAD_SIZE), f32),
            pltpu.VMEM((length, HEAD_SIZE), f32),
            pltpu.VMEM((16, length), f32),
            pltpu.VMEM((group_size, 16, length), f32),
            pltpu.VMEM((length, 2 * HEAD_SIZE), bf),
            pltpu.VMEM((rows, group_size * 2 * HEAD_SIZE), bf),
            pltpu.VMEM((length // BLOCK, HEAD_SIZE, 2 * HEAD_SIZE), f32),
            pltpu.VMEM((1, HEAD_SIZE, HEAD_SIZE), f32),
            dma((npair,)), dma((group * ntp,)), dma((group * ntp,)),
            dma((npair,)), dma((npair,)),
            dma((group_size,)), dma((group_size,)), dma((group_size,)), dma((group_size,)), dma((1,)),
        ],
        proj, extra_all,
        *(
            a.reshape(1, -1)
            for a in (key_gain, removal_gain, removal_bias, decay_bias, scan_norm_gain, conv_bias, conv_norm_gain)
        ),
        conv_kernel, outw,
    )


def solution(mesh):
    two = P("sp", "tp")
    one = P("tp")
    placed = (
        two, P(), two, two, two, two, two, two, one, one, one, one, two, one,
        two, two, P(None, "tp"), one, one, P("tp", "sp"), P("tp", "sp"),
    )
    return jax.shard_map(shards, mesh=mesh, in_specs=placed, out_specs=two, check_vma=False)
```

time: 143 us -> 97.8 us (0.68)
  matrix products: 19 us -> 0 us
  local copies, waits for them, and re-layouts: 21.3 us -> 6.51 us
  Pallas kernels: 97.5 us -> 90.6 us
  other arithmetic: 3.12 us -> 0.08 us
    dot_general x44 -> x0, matrix products: 19 us -> none  [the longest x9 6.96 us: matmul(): return jnp.dot(left, right, precision=exact_setting)]
    unnamed x88 -> x39, local copies, waits for them, and re-layouts: 15.3 us -> 4.6 us
    pallas_call x3 -> x2, Pallas kernels: 97.5 us -> 90.6 us  [call(): pl.pallas_call(kernel, out_shape=outs, in_specs=[vmem] * len(operands), o...]
where the time goes in v2:
time: 97.8 us; the launch traced here: 97.4 us
  Pallas kernels  90.6 us (93%)
  local copies, waits for them, and re-layouts  6.51 us (7%)
    pallas_call x2, Pallas kernels, call(): pl.pallas_call(kernel, out_shape=outs, in_specs=[vmem] * len(operands), o...  90.6 us
    unnamed x39, local copies, waits for them, and re-layouts  4.6 us

profile of v2, /device:TPU:0, one launch (start us, length us, event | category | flops | bytes accessed | tf_op | source)
XLA Modules:
  0.0 97.4 jit_solution(15196547030186345530)
XLA Ops:
  0.0 0.0 copy-start.11
  0.0 0.0 copy-start.12
  0.0 1.1 %fusion.2 = (bf16[256,64]{1,0:T(8,128)(2,1)S(1)}, bf16[256,64]{1,0:T(8,128)(2,1)S(1)}, bf16[256,64]{1,0:T(8,128)(2,1)S(1)}, bf16[256,64]{1,0:T(8,128)(2,1)S(1)}) fusion(bf16[256,128]{1,0:T(8,128)(2,1)} %param.36, bf16[256,128]{1,0:T(8,128)(2,1)} %param.35), kind=kLoop, calls=%fused_computation.7 | loop fusion | bytes 262144 | tf_op jit(solution)/shard_map/slice | solution.py:524
  1.1 0.0 copy-done.11
  1.1 0.0 copy-done.12
  1.1 0.0 copy-start.13
  1.1 0.0 copy-start.14
  1.1 0.1 fusion.4
  1.2 0.7 copy-done.13
  1.9 0.0 copy-done.14
  2.0 0.0 copy-start.15
  2.0 0.0 copy-start.16
  2.0 0.1 fusion.6
  2.1 0.7 copy-done.15
  2.8 0.0 copy-done.16
  2.9 0.1 fusion.8
  3.0 0.2 concatenate.9
  3.2 0.2 concatenate.10
  3.4 0.0 copy-start.10
  3.4 0.1 pad_maximum_fusion.weights
  3.5 0.8 copy-done.10
  4.3 0.1 slice_bitcast_fusion.1
  4.4 0.0 copy-start
  4.4 0.0 copy-start.2
  4.4 0.9 copy-done
  5.3 0.0 copy-done.2
  5.3 0.0 copy-start.17
  5.3 0.0 copy-start.18
  5.3 58.4 %shard_map.199 = (bf16[416,512]{1,0:T(8,128)(2,1)S(1)}, f32[2,192,64]{2,1,0:T(8,128)S(1)}) custom-call(bf16[192,512]{1,0:T(8,128)(2,1)S(1)} %copy-done, f32[1,2048]{1,0:T(1,128)S(1)} %bitcast.14, bf16[2,256,512]{2,1,0:T(8,128)(2,1)S(1)} %pad_maximum_fusion.weights, f32[2,192,64]{2,1,0:T(8,128)S(1)} %pad_maximum_fusion.1.extra), custom_call_target="tpu_custom_call" | custom-call | tf_op jit(solution)/shard_map/pallas_call | solution.py:495
  63.7 0.0 copy-done.17
  63.7 0.0 copy-done.18
  63.8 0.0 copy-start.1
  63.8 0.0 copy-start.6
  63.8 0.0 copy-start.7
  63.8 0.0 copy-start.8
  63.8 0.0 copy-start.9
  63.8 0.0 copy-start.3
  63.9 0.0 copy-start.4
  63.9 0.0 copy-start.5
  63.9 0.6 copy-done.1
  64.5 0.0 copy-done.6
  64.5 0.0 copy-done.7
  64.5 0.0 copy-done.8
  64.5 0.0 copy-done.9
  64.5 0.0 copy-done.3
  64.5 0.0 copy-done.4
  64.5 0.0 copy-done.5
  64.5 32.2 %shard_map.200 = bf16[192,512]{1,0:T(8,128)(2,1)S(1)} custom-call(bf16[416,512]{1,0:T(8,128)(2,1)S(1)} %get-tuple-element.7.proj, f32[2,192,64]{2,1,0:T(8,128)S(1)} %get-tuple-element.8.extra, f32[1,128]{1,0:T(1,128)S(1)} %bitcast.15, f32[1,128]{1,0:T(1,128)S(1)} %bitcast.16, f32[1,128]{1,0:T(1,128)S(1)} %bitcast.17, f32[1,128]{1,0:T(1,128)S(1)} %bitcast.18, ...), custom_call_target="tpu_custom_call" | custom-call | tf_op jit(solution)/shard_map/pallas_call | solution.py:495
  96.7 0.7 copy.23
  (3 shorter events, 0.0 us)
Async XLA Ops:
  0.0 1.1 %copy-start.11 = (bf16[256,128]{1,0:T(8,128)(2,1)S(1)}, bf16[256,128]{1,0:T(8,128)(2,1)}, u32[]{:S(2)}) copy-start(bf16[256,128]{1,0:T(8,128)(2,1)} %param.28) | copy-start | bytes 196612
  0.0 1.1 %copy-start.12 = (bf16[256,128]{1,0:T(8,128)(2,1)S(1)}, bf16[256,128]{1,0:T(8,128)(2,1)}, u32[]{:S(2)}) copy-start(bf16[256,128]{1,0:T(8,128)(2,1)} %param.27) | copy-start | bytes 196612
  1.1 0.8 copy-start.13
  1.1 0.9 copy-start.14
  2.0 0.8 copy-start.15
  2.0 0.9 copy-start.16
  3.4 0.9 copy-start.10
  4.4 0.9 copy-start
  4.4 0.9 copy-start.2
  5.3 58.4 %copy-start.17 = (bf16[128,256]{1,0:T(8,128)(2,1)S(1)}, bf16[128,256]{1,0:T(8,128)(2,1)}, u32[]{:S(2)}) copy-start(bf16[128,256]{1,0:T(8,128)(2,1)} %param.40) | copy-start | bytes 196612
  5.3 58.4 %copy-start.18 = (bf16[128,256]{1,0:T(8,128)(2,1)S(1)}, bf16[128,256]{1,0:T(8,128)(2,1)}, u32[]{:S(2)}) copy-start(bf16[128,256]{1,0:T(8,128)(2,1)} %param.41) | copy-start | bytes 196612
  63.8 0.7 copy-start.1
  63.8 0.7 copy-start.6
  63.8 0.7 copy-start.7
  63.8 0.7 copy-start.8
  63.8 0.7 copy-start.9
  63.8 0.7 copy-start.3
  63.9 0.7 copy-start.4
  63.9 0.7 copy-start.5
